TPU v7x, 32 devices: a whole 2x2x4 slice. The times are simulated.
32 devices in a mesh: fs: 8 (over z, x), tp: 4 (over y, core).
Axes of the slice: x: 2, y: 2, z: 4, core: 2. Of those that a mesh axis runs over, the one named last changes fastest.
Arguments:
- normed_input: bfloat16 [16384, 2048], P('fs'), may hold values from -6 to 6
- output_cotangent: bfloat16 [16384, 2048], P('fs'), may hold values from -6 to 6
- query_grad: bfloat16 [16384, 2048], P('fs', 'tp'), may hold values from -0.75 to 0.75
- key_grad: bfloat16 [16384, 2048], P('fs', 'tp'), may hold values from -0.75 to 0.75
- attn_values: bfloat16 [16384, 2048], P('fs', 'tp'), may hold values from -0.75 to 0.75
- master_weights: float32 [3, 2048, 2048], P(None, 'fs', 'tp'), may hold values from -3 to 3
- factors: bfloat16 [3, 2048, 256], P(None, 'fs'), may hold values from -0.375 to 0.375
- moments: float32 [3, 256, 2048], P(None, 'fs', 'tp'), may hold values from -620 to 620
Outputs:
- new_weights: float32 [3, 2048, 2048], P(None, 'fs', 'tp')
- weight_copies: bfloat16 [3, 2048, 2048], P(None, None, 'tp')
- steps: float32 [3, 2048, 2048], P(None, 'fs', 'tp')
- new_moments: float32 [3, 256, 2048], P(None, 'fs', 'tp')
All inputs are finite; a program needn't handle non-finite values.
Results may differ from a plain program's by a relative error of at most 0.0055.
Values may be sent and summed in bfloat16 or wider, within the bound.
A program may use at most 128 MiB of HBM per device.

v0:
```python
import jax
import jax.numpy as jnp
from jax import lax
from jax.sharding import PartitionSpec as P


def on_device(
    normed_input,
    output_cotangent,
    query_grad,
    key_grad,
    attn_values,
    master_weights,
    factors,
    moments,
):
    rank_rows = moments.shape[1]
    width = query_grad.shape[1]
    rank = factors.shape[2]
    contract = (((0,), (0,)), ((), ()))
    whole_factors = lax.all_gather(factors, "fs", axis=1, tiled=True)
    reduced = [
        jnp.dot(normed_input, whole_factors[0], preferred_element_type=jnp.float32),
        jnp.dot(normed_input, whole_factors[1], preferred_element_type=jnp.float32),
        jnp.dot(output_cotangent, whole_factors[2], preferred_element_type=jnp.float32),
    ]
    head_sides = [query_grad, key_grad, attn_values]
    pieces = []
    for index in range(3):
        reduced_cols = reduced[index]
        pieces.append(
            lax.dot_general(
                reduced_cols,
                head_sides[index].astype(jnp.float32),
                contract,
                precision=lax.Precision.HIGHEST,
                preferred_element_type=jnp.float32,
            )
        )
    projected = lax.psum_scatter(
        jnp.concatenate(pieces, axis=1).astype(jnp.bfloat16), "fs", scatter_dimension=0, tiled=True
    ).astype(jnp.float32)
    split = projected.reshape(rank_rows, 3, width).transpose(1, 0, 2)
    new_moments = 0.8 * moments + 0.2 * split
    total = lax.psum(jnp.sum(new_moments * new_moments), ("fs", "tp"))
    entries = 3 * rank * width * lax.axis_size("tp")
    rms = jnp.sqrt(total / entries + 1e-06)
    normalized = (new_moments / rms).astype(jnp.bfloat16)
    gathered = lax.all_gather(normalized, "fs", axis=1, tiled=True)
    steps = jnp.einsum("jdr,jrc->jdc", factors, gathered, preferred_element_type=jnp.float32)
    new_weights = master_weights - 0.05 * steps
    weight_copies = lax.all_gather(new_weights.astype(jnp.bfloat16), "fs", axis=1, tiled=True)
    return (new_weights, weight_copies, steps, new_moments)


def solution(mesh):
    in_specs = (
        P("fs", None),
        P("fs", None),
        P("fs", "tp"),
        P("fs", "tp"),
        P("fs", "tp"),
        P(None, "fs", "tp"),
        P(None, "fs", None),
        P(None, "fs", "tp"),
    )
    out_specs = (P(None, "fs", "tp"), P(None, None, "tp"), P(None, "fs", "tp"), P(None, "fs", "tp"))
    return jax.shard_map(
        on_device, mesh=mesh, in_specs=in_specs, out_specs=out_specs, check_vma=False
    )
```

profile of v0, /device:TPU:0, one launch (start us, length us, event | category | flops | bytes accessed | tf_op | source)
XLA Modules:
  0.0 345.6 jit_solution(5577929369961026899)
XLA Ops:
  7.2 0.0 copy-start
  7.2 0.0 all-gather.3.cloned.1.call-start
  7.2 0.7 all-gather.3.cloned.1.call-update
  7.9 0.0 reduce-scatter.2.cloned.1.call-start
  8.0 65.0 %all-gather.3.cloned.1.call-done = bf16[3,2048,256]{2,1,0:T(8,128)(2,1)} async-done(((bf16[3,256,256]{2,1,0:T(8,128)(2,1)}), bf16[3,2048,256]{2,1,0:T(8,128)(2,1)}) %all-gather.3.cloned.1.call-update) | async-done | bytes 3145744 | tf_op jit(solution)/shard_map/all_gather | solution.py:21
  72.9 0.0 copy-start.6
  72.9 6.2 %fusion = f32[2048,256]{1,0:T(8,128)S(1)} fusion(bf16[2048,2048]{1,0:T(8,128)(2,1)} %param.9, bf16[3,2048,256]{2,1,0:T(8,128)(2,1)} %all-gather.3.cloned.1.call-done), kind=kOutput, calls=%fused_computation.6 | convolution fusion | flops 2147483648 | bytes 11534336 | tf_op jit(solution)/shard_map/dot_general | solution.py:25
  79.2 0.0 copy-done
  79.2 0.0 copy-start.7
  79.2 1.9 convolution_convert_fusion
  81.2 0.0 copy-done.6
  81.2 0.0 copy-done.7
  81.2 0.0 copy-start.1
  81.2 2.5 fusion.1
  83.7 0.0 copy-done.1
  83.7 1.8 convolution_convert_fusion.1
  85.5 0.0 copy-start.2
  85.5 2.5 fusion.2
  88.0 0.0 copy-done.2
  88.0 2.0 convolution_convert_fusion.2
  90.0 0.9 pad_maximum_fusion
  91.0 0.0 copy-start.5
  91.0 0.0 reduce-scatter.2.cloned.1.call-update
  91.0 0.0 copy-start.3
  91.0 0.0 all-gather.5.cloned.1.call-start
  91.1 3.1 copy.18
  94.2 58.9 %reduce-scatter.2.cloned.1.call-done = bf16[32,1536]{1,0:T(8,128)(2,1)} async-done(((bf16[256,1536]{1,0:T(8,128)(2,1)}), bf16[32,1536]{1,0:T(8,128)(2,1)}) %reduce-scatter.2.cloned.1.call-update) | async-done | bytes 98320 | tf_op jit(solution)/shard_map/reduce_scatter | solution.py:40
  153.1 0.9 convert_multiply_fusion
  154.0 0.0 copy-done.5
  154.0 0.7 multiply_reduce_fusion
  154.7 0.0 copy-start.4
  154.7 40.0 %psum.7 = f32[]{:T(128)} all-reduce(f32[]{:T(128)} %get-tuple-element.14), channel_id=1, replica_groups=mesh['fs'=8,'tp'=4] {'fs','tp'}, use_global_device_ids=true, to_apply=%region_2.0 | all-reduce | flops 1 | bytes 8 | tf_op jit(solution)/shard_map/psum | solution.py:45
  195.4 32.0 %all_gather.10 = bf16[3,256,512]{2,1,0:T(8,128)(2,1)S(1)} all-gather(bf16[3,32,512]{2,1,0:T(8,128)(2,1)S(1)} %divide_convert_fusion), channel_id=1, replica_groups=mesh['fs'=8,'tp'=4] {'fs'}, dimensions={1}, use_global_device_ids=true | all-gather | bytes 884736 | tf_op jit(solution)/shard_map/all_gather | solution.py:49
  227.5 0.0 copy-done.3
  227.5 3.9 %fusion.4 = (bf16[3,256,512]{1,2,0:T(8,128)(2,1)}, f32[3,256,512]{1,2,0:T(8,128)}, f32[3,256,512]{1,2,0:T(8,128)}) fusion(f32[3,256,512]{1,2,0:T(8,128)} %copy.18, bf16[3,256,512]{2,1,0:T(8,128)(2,1)S(1)} %all_gather.10, bf16[3,256,256]{2,1,0:T(8,128)(2,1)S(1)} %copy-done.3), kind=kOutput, calls=%fused_computation.17 | convolution fusion | flops 202506240 | bytes 6684672 | tf_op jit(solution)/shard_map/jdr,jrc->jdc/dot_general | solution.py:50
  231.3 0.0 copy-done.4
  231.3 0.0 all-gather.5.cloned.1.call-update
  231.4 3.0 copy.19
  234.4 3.0 copy.21
  237.4 93.1 %all-gather.5.cloned.1.call-done = bf16[3,2048,512]{1,2,0:T(8,128)(2,1)} async-done(((bf16[3,256,512]{1,2,0:T(8,128)(2,1)}), bf16[3,2048,512]{1,2,0:T(8,128)(2,1)}) %all-gather.5.cloned.1.call-update) | async-done | bytes 6291472 | tf_op jit(solution)/shard_map/all_gather | solution.py:52
  330.5 8.6 %copy.20 = bf16[3,2048,512]{2,1,0:T(8,128)(2,1)} copy(bf16[3,2048,512]{1,2,0:T(8,128)(2,1)} %all-gather.5.cloned.1.call-done) | data formatting | bytes 12582912
  (1 shorter events, 0.0 us)
Async XLA Ops:
  7.2 72.0 %copy-start = (bf16[2048,512]{1,0:T(8,128)(2,1)S(1)}, bf16[2048,512]{1,0:T(8,128)(2,1)}, u32[]{:S(2)}) copy-start(bf16[2048,512]{1,0:T(8,128)(2,1)} %param.12) | copy-start | bytes 6291460
  7.2 65.8 %all-gather.3.cloned.1.call-start = ((), (), s32[]{:S(2)}) async-start(), calls=%async_computation.1 | async-start | bytes 3538944 | tf_op jit(solution)/shard_map/all_gather | solution.py:21
  7.9 145.2 %reduce-scatter.2.cloned.1.call-start = ((), (), s32[]{:S(2)}) async-start(), calls=%async_computation.2 | async-start | bytes 884736 | tf_op jit(solution)/shard_map/reduce_scatter | solution.py:40
  72.9 8.2 %copy-start.6 = (bf16[2048,2048]{1,0:T(8,128)(2,1)S(1)}, bf16[2048,2048]{1,0:T(8,128)(2,1)}, u32[]{:S(2)}) copy-start(bf16[2048,2048]{1,0:T(8,128)(2,1)} %param.8) | copy-start | bytes 25165828
  79.2 2.0 copy-start.7
  81.2 2.5 copy-start.1
  85.5 2.5 copy-start.2
  91.0 63.0 %copy-start.5 = (f32[3,32,512]{2,1,0:T(8,128)S(1)}, f32[3,32,512]{2,1,0:T(8,128)}, u32[]{:S(2)}) copy-start(f32[3,32,512]{2,1,0:T(8,128)} %param.15) | copy-start | bytes 589828
  91.0 136.5 %copy-start.3 = (bf16[3,256,256]{2,1,0:T(8,128)(2,1)S(1)}, bf16[3,256,256]{2,1,0:T(8,128)(2,1)}, u32[]{:S(2)}) copy-start(bf16[3,256,256]{2,1,0:T(8,128)(2,1)} %param.14) | copy-start | bytes 1179652
  91.0 239.5 %all-gather.5.cloned.1.call-start = ((), (), s32[]{:S(2)}) async-start(), calls=%async_computation.3 | async-start | bytes 7077888 | tf_op jit(solution)/shard_map/all_gather | solution.py:52
  154.7 76.7 %copy-start.4 = (f32[3,32,512]{2,1,0:T(8,128)}, f32[3,32,512]{2,1,0:T(8,128)S(1)}, u32[]{:S(2)}) copy-start(f32[3,32,512]{2,1,0:T(8,128)S(1)} %get-tuple-element.15) | copy-start | bytes 589828
Sparse Core Ops, SparseCore 0:
  10.2 62.7 all-gather.2
  91.1 61.9 reduce-scatter.1
  231.5 98.9 all-gather.4
where the time goes:
time: 346 us
  waiting for transfers between devices  218 us (63%)
  blocking collectives  72.1 us (21%)
  matrix products  20.8 us (6%)
  local copies, waits for them, and re-layouts  17.8 us (5%)
  between operations  14.6 us (4%)
    all_gather x1, waiting for transfers between devices, on_device(): lax.all_gather(new_weights.astype(jnp.bfloat16), 'fs', axis=1, tiled=True)  93.1 us
    all_gather x1, waiting for transfers between devices, on_device(): whole_factors = lax.all_gather(factors, 'fs', axis=1, tiled=True)  65 us
    reduce_scatter x1, waiting for transfers between devices, on_device(): lax.psum_scatter(jnp.concatenate(pieces, axis=1).astype(jnp.bfloat16), 'f...  58.9 us
    psum x1, blocking collectives, on_device(): total = lax.psum(jnp.sum(new_moments * new_moments), ('fs', 'tp'))  40 us
    all_gather x1, blocking collectives, on_device(): gathered = lax.all_gather(normalized, 'fs', axis=1, tiled=True)  32 us
    unnamed x20, local copies, waits for them, and re-layouts  17.8 us
  transfers between devices with their start and end apart: 3, of which 3 were waited for; matrix products, arithmetic and copies ran while one was open for 3% of the time, Pallas kernels for 0%

commit v1 on v0

v1 whole, which is shorter than its diff:
```python
import functools

import jax
import jax.numpy as jnp
from jax import lax
from jax.experimental import pallas as pl
from jax.experimental.pallas import tpu as pltpu
from jax.sharding import PartitionSpec as P

MESH = pl.DeviceIdType.MESH
F32 = jnp.float32
BF16 = jnp.bfloat16


def grid_of(count):
    cols = 1
    while cols * cols * 4 <= count:
        cols *= 2
    return count // cols, cols


class Relay:
    def __init__(self, own, slot, send, recv, first, second, dev, hook=None, hook_drain=None):
        self.own, self.slot, self.send, self.recv = own, slot, send, recv
        (self.a, self.na), (self.b, self.nb) = first, second
        self.dev, self.hook, self.hook_drain = dev, hook, hook_drain
        a, b = self.a, self.b
        self.open = [a + 1 < self.na, a >= 1, b + 1 < self.nb, b >= 1]
        self.target = [(a + 1, b), (a - 1, b), (a, b + 1), (a, b - 1)]
        self.sent = []
        self.steps = [self.start]
        self.steps += [functools.partial(self.along_first, k) for k in range(1, self.na)]
        self.steps += [functools.partial(self.along_second, k) for k in range(1, self.nb)]
        self.at = 0

    def copy(self, owner, way, src):
        return pltpu.make_async_remote_copy(
            src_ref=src,
            dst_ref=self.slot(owner),
            send_sem=self.send.at[owner, way],
            recv_sem=self.recv.at[owner],
            device_id={"fs": self.dev(*self.target[way])},
            device_id_type=MESH,
        )

    def push(self, cond, owner, way, src):
        both = self.open[way] if cond is None else jnp.logical_and(cond, self.open[way])
        self.sent.append((both, owner, way, src))

        @pl.when(both)
        def _():
            self.copy(owner, way, src).start()

    def arrive(self, cond, owner, ways, came):
        @pl.when(cond)
        def _():
            self.copy(owner, came, self.slot(owner)).wait_recv()

        for way in ways:
            self.push(cond, owner, way, self.slot(owner))
        if self.hook is not None:

            @pl.when(cond)
            def _():
                self.hook(owner)

    def start(self):
        me = self.dev(self.a, self.b)
        for way in range(4):
            self.push(None, me, way, self.own)

    def along_first(self, k):
        self.arrive(self.a >= k, self.dev(self.a - k, self.b), (0, 2, 3), 1)
        self.arrive(self.a + k < self.na, self.dev(self.a + k, self.b), (1, 2, 3), 0)

    def along_second(self, k):
        for row in range(self.na):
            self.arrive(self.b >= k, self.dev(row, self.b - k), (2,), 3)
            self.arrive(self.b + k < self.nb, self.dev(row, self.b + k), (3,), 2)

    def tick(self, count=1):
        for _ in range(count):
            if self.at < len(self.steps):
                self.steps[self.at]()
                self.at += 1

    def finish(self):
        self.tick(len(self.steps))

    def drain(self):
        for cond, owner, way, src in self.sent:

            @pl.when(cond)
            def _():
                self.copy(owner, way, src).wait_send()


def exchange_kernel(
    nfs, ntp,
    x_in, o_in, q_in, k_in, v_in, w_in, p_in, m_ref,
    wfull, pfull, nmfull, new_m, total,
    xbuf, ybuf, sacc, sbuf, rbuf, tbuf, ubuf,
    load_sem, p_send, p_recv, d_send, d_recv, w_send, w_recv, n_send, n_recv,
    r_send, r_recv, t_send, t_recv, u_send, u_recv,
):
    me = lax.axis_index("fs")
    tp = lax.axis_index("tp")
    nz, nx = grid_of(nfs)
    z, x = me // nx, me % nx
    core = tp % 2
    mate = tp + 1 - 2 * core
    block = p_in.shape[1]
    half = block // 2
    rr = m_ref.shape[1]

    loads = [
        pltpu.make_async_copy(p_in, pfull.at[:, pl.ds(pl.multiple_of(me * block, block), block), :], load_sem.at[0]),
        pltpu.make_async_copy(x_in, xbuf.at[0], load_sem.at[1]),
        pltpu.make_async_copy(q_in, ybuf.at[0], load_sem.at[2]),
        pltpu.make_async_copy(k_in, ybuf.at[1], load_sem.at[3]),
        pltpu.make_async_copy(o_in, xbuf.at[1], load_sem.at[4]),
        pltpu.make_async_copy(v_in, ybuf.at[2], load_sem.at[5]),
    ]

    def zx(row, col):
        return row * nx + col

    def xz(col, row):
        return row * nx + col

    def p_slot(owner, which):
        return pfull.at[:, pl.ds(pl.multiple_of(owner * block + which * half, half), half), :]

    def mate_copy(owner, which):
        return pltpu.make_async_remote_copy(
            src_ref=p_slot(owner, which),
            dst_ref=p_slot(owner, which),
            send_sem=d_send.at[owner],
            recv_sem=d_recv.at[owner],
            device_id={"tp": mate},
            device_id_type=MESH,
        )

    factors = Relay(
        p_in.at[:, pl.ds(pl.multiple_of(core * half, half), half), :],
        lambda owner: p_slot(owner, core),
        p_send, p_recv, (z, nz), (x, nx), zx,
        hook=lambda owner: mate_copy(owner, core).start(),
    )

    def w_piece(index, j, low, size, across):
        def slot(owner):
            return wfull.at[j, pl.ds(pl.multiple_of(owner * block + low, half), size), :]

        first, second, dev = ((x, nx), (z, nz), xz) if across else ((z, nz), (x, nx), zx)
        return Relay(
            w_in.at[j, pl.ds(low, size), :], slot, w_send.at[index], w_recv.at[index], first, second, dev
        )

    weights = [
        w_piece(0, 0, 0, block, False),
        w_piece(1, 1, 0, block, False),
        w_piece(2, 2, 0, half, False),
        w_piece(3, 2, half, half, True),
    ]

    def n_slot(owner):
        return nmfull.at[:, pl.ds(pl.multiple_of(owner * rr, rr), rr), :]

    momentum = Relay(n_slot(me), n_slot, n_send, n_recv, (z, nz), (x, nx), zx)

    factors.tick()
    for load in loads:
        load.start()
    factors.tick(2)
    weights[0].tick()
    factors.finish()
    weights[0].tick()
    weights[3].tick()
    loads[0].wait()
    for m in range(1, nfs):
        owner = lax.rem(me + m, nfs)
        mate_copy(owner, 1 - core).wait_recv()

    tokens = xbuf.shape[1]
    tile = min(256, tokens)

    def scatter_copy(j, m):
        to = lax.rem(me + m, nfs)
        return pltpu.make_async_remote_copy(
            src_ref=sbuf.at[j, pl.ds(pl.multiple_of(to * rr, rr), rr), :],
            dst_ref=rbuf.at[m, j],
            send_sem=r_send.at[m, j],
            recv_sem=r_recv.at[m, j],
            device_id={"fs": to},
            device_id_type=MESH,
        )

    def project(j, side):
        sacc[...] = jnp.zeros_like(sacc)

        @pl.loop(0, tokens // tile)
        def _(t):
            rows = pl.ds(pl.multiple_of(t * tile, tile), tile)
            reduced = jnp.dot(xbuf[side, rows, :], pfull[j], preferred_element_type=F32)
            sacc[...] += lax.dot_general(
                reduced.astype(BF16), ybuf[j, rows, :], (((0,), (0,)), ((), ())), preferred_element_type=F32
            )

        sbuf[j] = sacc[...].astype(BF16)

    loads[1].wait()
    loads[2].wait()
    project(0, 0)
    weights[0].tick()
    weights[3].tick()
    for m in range(1, nfs):
        scatter_copy(0, m).start()
    weights[1].tick()
    loads[3].wait()
    project(1, 0)
    for m in range(1, nfs):
        scatter_copy(1, m).start()
    weights[0].tick()
    weights[1].tick()
    weights[3].tick()
    loads[4].wait()
    loads[5].wait()
    project(2, 1)
    for m in range(1, nfs):
        scatter_copy(2, m).start()
    weights[2].tick()
    weights[1].tick()
    weights[3].tick()

    squares = jnp.zeros((), F32)
    for j in range(3):
        value = sbuf[j, pl.ds(pl.multiple_of(me * rr, rr), rr), :].astype(F32)
        for m in range(1, nfs):
            scatter_copy(j, m).wait_recv()
            value = value + rbuf[m, j].astype(F32)
        fresh = 0.8 * m_ref[j] + 0.2 * value
        new_m[j] = fresh
        nmfull[j, pl.ds(pl.multiple_of(me * rr, rr), rr), :] = fresh.astype(BF16)
        squares = squares + jnp.sum(fresh * fresh)
    tbuf[0] = jnp.full(tbuf.shape[1:], squares, F32)

    def spread(buf, send, recv, axis, size, m):
        to = lax.rem(lax.axis_index(axis) + m, size)
        return pltpu.make_async_remote_copy(
            src_ref=buf.at[0],
            dst_ref=buf.at[m],
            send_sem=send.at[m],
            recv_sem=recv.at[m],
            device_id={axis: to},
            device_id_type=MESH,
        )

    momentum.tick()
    for m in range(1, nfs):
        spread(tbuf, t_send, t_recv, "fs", nfs, m).start()
    momentum.tick()
    part = tbuf[0]
    for m in range(1, nfs):
        spread(tbuf, t_send, t_recv, "fs", nfs, m).wait_recv()
        part = part + tbuf[m]
    ubuf[0] = part
    for m in range(1, ntp):
        spread(ubuf, u_send, u_recv, "tp", ntp, m).start()
    momentum.tick()
    weights[1].tick()
    weights[2].tick()
    momentum.tick()
    weights[3].tick()
    weights[2].tick()
    whole = part
    for m in range(1, ntp):
        spread(ubuf, u_send, u_recv, "tp", ntp, m).wait_recv()
        whole = whole + ubuf[m]
    total[...] = whole
    weights[2].tick()
    momentum.finish()
    for piece in weights:
        piece.finish()

    factors.drain()
    momentum.drain()
    for piece in weights:
        piece.drain()
    for m in range(1, nfs):
        owner = lax.rem(me + m, nfs)
        mate_copy(owner, core).wait_send()
        for j in range(3):
            scatter_copy(j, m).wait_send()
        spread(tbuf, t_send, t_recv, "fs", nfs, m).wait_send()
    for m in range(1, ntp):
        spread(ubuf, u_send, u_recv, "tp", ntp, m).wait_send()


def exchange(nfs, ntp, x, o, q, k, v, w16, p, m):
    block, rank = p.shape[1], p.shape[2]
    rr, cols = m.shape[1], m.shape[2]
    tokens, model = x.shape
    anywhere = pl.BlockSpec(memory_space=pl.ANY)
    vmem = pl.BlockSpec(memory_space=pltpu.VMEM)
    dma = pltpu.SemaphoreType.DMA
    return pl.pallas_call(
        functools.partial(exchange_kernel, nfs, ntp),
        out_shape=(
            jax.ShapeDtypeStruct((3, nfs * block, cols), BF16),
            jax.ShapeDtypeStruct((3, nfs * block, rank), BF16),
            jax.ShapeDtypeStruct((3, rank, cols), BF16),
            jax.ShapeDtypeStruct(m.shape, F32),
            jax.ShapeDtypeStruct((8, 128), F32),
        ),
        in_specs=[anywhere] * 7 + [vmem],
        out_specs=(anywhere, vmem, vmem, vmem, vmem),
        scratch_shapes=[
            pltpu.VMEM((2, tokens, model), BF16),
            pltpu.VMEM((3, tokens, cols), BF16),
            pltpu.VMEM((rank, cols), F32),
            pltpu.VMEM((3, rank, cols), BF16),
            pltpu.VMEM((nfs, 3, rr, cols), BF16),
            pltpu.VMEM((nfs, 8, 128), F32),
            pltpu.VMEM((ntp, 8, 128), F32),
            dma((6,)),
            dma((nfs, 4)), dma((nfs,)),
            dma((nfs,)), dma((nfs,)),
            dma((4, nfs, 4)), dma((4, nfs)),
            dma((nfs, 4)), dma((nfs,)),
            dma((nfs, 3)), dma((nfs, 3)),
            dma((nfs,)), dma((nfs,)),
            dma((ntp,)), dma((ntp,)),
        ],
        compiler_params=pltpu.CompilerParams(has_side_effects=True, vmem_limit_bytes=56 * 2**20),
        cost_estimate=pl.CostEstimate(flops=8 * 10**9, bytes_accessed=40 * 10**6, transcendentals=0),
        name="exchange",
    )(x, o, q, k, v, w16, p, m)


def update_kernel(nfs, entries, w_ref, p_ref, n_ref, t_ref, master_ref, m_ref, nw_ref, copies_ref, steps_ref, mo_ref):
    step_at = pl.program_id(0)
    me = lax.axis_index("fs")
    scale = 1.0 / jnp.sqrt(t_ref[0:1, 0:1] / entries + 1e-06)
    for j in range(3):
        step = jnp.dot(p_ref[j], n_ref[j], preferred_element_type=F32) * scale

        @pl.when(step_at == me)
        def _():
            steps_ref[j] = step
            fresh = master_ref[j] - 0.05 * step
            nw_ref[j] = fresh
            copies_ref[j] = fresh.astype(BF16)
            mo_ref[j] = m_ref[j]

        @pl.when(step_at != me)
        def _():
            copies_ref[j] = (w_ref[j].astype(F32) - 0.05 * step).astype(BF16)


def update(nfs, ntp, wfull, pfull, nmfull, total, master, new_m):
    block, cols = master.shape[1], master.shape[2]
    rank = nmfull.shape[1]
    entries = float(3 * rank * cols * ntp)
    whole = lambda a: pl.BlockSpec(a.shape, lambda b: (0,) * a.ndim)
    per_block = lambda width: pl.BlockSpec((3, block, width), lambda b: (0, b, 0))
    return pl.pallas_call(
        functools.partial(update_kernel, nfs, entries),
        grid=(nfs,),
        out_shape=(
            jax.ShapeDtypeStruct(master.shape, F32),
            jax.ShapeDtypeStruct(wfull.shape, BF16),
            jax.ShapeDtypeStruct(master.shape, F32),
            jax.ShapeDtypeStruct(new_m.shape, F32),
        ),
        in_specs=[per_block(cols), per_block(rank), whole(nmfull), whole(total), whole(master), whole(new_m)],
        out_specs=(whole(master), per_block(cols), whole(master), whole(new_m)),
        compiler_params=pltpu.CompilerParams(dimension_semantics=("arbitrary",)),
        cost_estimate=pl.CostEstimate(flops=2 * 10**9, bytes_accessed=20 * 10**6, transcendentals=0),
        name="update",
    )(wfull, pfull, nmfull, total, master, new_m)


def solution(mesh):
    nfs, ntp = mesh.shape["fs"], mesh.shape["tp"]

    def on_device(x, o, q, k, v, master, p, m):
        wfull, pfull, nmfull, new_m, total = exchange(nfs, ntp, x, o, q, k, v, master.astype(BF16), p, m)
        return update(nfs, ntp, wfull, pfull, nmfull, total, master, new_m)

    in_specs = (
        P("fs", None),
        P("fs", None),
        P("fs", "tp"),
        P("fs", "tp"),
        P("fs", "tp"),
        P(None, "fs", "tp"),
        P(None, "fs", None),
        P(None, "fs", "tp"),
    )
    out_specs = (P(None, "fs", "tp"), P(None, None, "tp"), P(None, "fs", "tp"), P(None, "fs", "tp"))
    return jax.shard_map(
        on_device, mesh=mesh, in_specs=in_specs, out_specs=out_specs, check_vma=False
    )
```

time: 346 us -> 144 us (0.42)
  waiting for transfers between devices: 218 us -> 0 us
  Pallas kernels: 0 us -> 141 us
  blocking collectives: 72.1 us -> 0 us
  matrix products: 20.8 us -> 0 us
  local copies, waits for them, and re-layouts: 17.8 us -> 0 us
  between operations: 14.6 us -> 0.64 us
    all_gather x2 -> x0, waiting for transfers between devices: 158 us -> none  [the longest x1 93.1 us: on_device(): lax.all_gather(new_weights.astype(jnp.bfloat16), 'fs', axis=1, tiled=True)]
    pallas_call x0 -> x2, Pallas kernels: none -> 141 us  [the longest x1 127 us: exchange(): pl.pallas_call(functools.partial(exchange_kernel, nfs, ntp), out_shape=(j...]
    reduce_scatter x1 -> x0, waiting for transfers between devices: 58.9 us -> none  [on_device(): lax.psum_scatter(jnp.concatenate(pieces, axis=1).astype(jnp.bfloat16), 'f...]
    psum x1 -> x0, blocking collectives: 40 us -> none  [on_device(): total = lax.psum(jnp.sum(new_moments * new_moments), ('fs', 'tp'))]
    all_gather x1 -> x0, blocking collectives: 32 us -> none  [on_device(): gathered = lax.all_gather(normalized, 'fs', axis=1, tiled=True)]
    dot_general x7 -> x0, matrix products: 20.8 us -> none  [the longest x1 6.23 us: on_device(): jnp.dot(output_cotangent, whole_factors[2], preferred_element_type=jnp.fl...]
    unnamed x20 -> x0, local copies, waits for them, and re-layouts: 17.8 us -> none
  transfers between devices with their start and end apart: 3 -> 0, of which waited for: 3 -> 0; matrix products, arithmetic and copies ran while one was open for 3% -> 0% of each run, Pallas kernels for 0% -> 0%
where the time goes in v1:
time: 144 us
  Pallas kernels  141 us (98%)
  other arithmetic  2.39 us (2%)
    pallas_call x1, Pallas kernels, exchange(): pl.pallas_call(functools.partial(exchange_kernel, nfs, ntp), out_shape=(j...  127 us
    pallas_call x1, Pallas kernels, update(): pl.pallas_call(functools.partial(update_kernel, nfs, entries), grid=(nfs,...  13.5 us

profile of v1, /device:TPU:0, one launch (start us, length us, event | category | flops | bytes accessed | tf_op | source)
XLA Modules:
  0.0 144.0 jit_solution(1301652882317079066)
XLA Ops:
  0.6 2.4 %convert_element_type.3.w_in = bf16[3,256,512]{2,1,0:T(8,128)(2,1)} convert(f32[3,256,512]{2,1,0:T(8,128)} %master_ref.1) | non-fusion elementwise | flops 393216 | bytes 2359296 | tf_op jit(solution)/shard_map/convert_element_type | solution.py:388
  3.0 127.4 %exchange.1 = (bf16[3,2048,512]{2,1,0:T(8,128)(2,1)}, bf16[3,2048,256]{2,1,0:T(8,128)(2,1)}, bf16[3,256,512]{2,1,0:T(8,128)(2,1)}, f32[3,32,512]{2,1,0:T(8,128)}, f32[8,128]{1,0:T(8,128)}) custom-call(bf16[2048,2048]{1,0:T(8,128)(2,1)} %x_in.1, bf16[2048,2048]{1,0:T(8,128)(2,1)} %o_in.1, bf16[2048,512]{1,0:T(8,128)(2,1)} %q_in.1, bf16[2048,512]{1,0:T(8,128)(2,1)} %k_in.1, ...), custom_call_target="tpu_custom_call" | custom-call | flops 8000000000 | bytes 40000000 | tf_op jit(solution)/shard_map/exchange/pallas_call | solution.py:307
  130.4 13.5 %update.1 = (f32[3,256,512]{2,1,0:T(8,128)}, bf16[3,2048,512]{2,1,0:T(8,128)(2,1)}, f32[3,256,512]{2,1,0:T(8,128)}, f32[3,32,512]{2,1,0:T(8,128)}) custom-call(bf16[3,2048,512]{2,1,0:T(8,128)(2,1)} %get-tuple-element.9.w_ref, bf16[3,2048,256]{2,1,0:T(8,128)(2,1)} %get-tuple-element.10.p_ref, bf16[3,256,512]{2,1,0:T(8,128)(2,1)} %get-tuple-element.11.n_ref, ...), custom_call_target="tpu_custom_call" | custom-call | flops 2000000000 | bytes 20000000 | tf_op jit(solution)/shard_map/update/pallas_call | solution.py:367

commit v2 on v1

--- a/solution.py
+++ b/solution.py
@@ -10,6 +10,8 @@
 MESH = pl.DeviceIdType.MESH
 F32 = jnp.float32
 BF16 = jnp.bfloat16
+PITCH = 0.5
+PACE = (3, 3, 4, 6, 2, 2, 2, 2)
 
 
 def grid_of(count):
@@ -99,7 +101,7 @@
     nfs, ntp,
     x_in, o_in, q_in, k_in, v_in, w_in, p_in, m_ref,
     wfull, pfull, nmfull, new_m, total,
-    xbuf, ybuf, sacc, sbuf, rbuf, tbuf, ubuf,
+    xbuf, ybuf, wbuf, w16, sacc, sbuf, rbuf, tbuf, ubuf,
     load_sem, p_send, p_recv, d_send, d_recv, w_send, w_recv, n_send, n_recv,
     r_send, r_recv, t_send, t_recv, u_send, u_recv,
 ):
@@ -113,6 +115,12 @@
     half = block // 2
     rr = m_ref.shape[1]
 
+    barrier = pltpu.get_barrier_semaphore()
+    for m in range(1, nfs):
+        pl.semaphore_signal(barrier, inc=1, device_id={"fs": lax.rem(me + m, nfs)}, device_id_type=MESH)
+    for m in range(1, ntp):
+        pl.semaphore_signal(barrier, inc=1, device_id={"tp": lax.rem(tp + m, ntp)}, device_id_type=MESH)
+
     loads = [
         pltpu.make_async_copy(p_in, pfull.at[:, pl.ds(pl.multiple_of(me * block, block), block), :], load_sem.at[0]),
         pltpu.make_async_copy(x_in, xbuf.at[0], load_sem.at[1]),
@@ -120,6 +128,7 @@
         pltpu.make_async_copy(k_in, ybuf.at[1], load_sem.at[3]),
         pltpu.make_async_copy(o_in, xbuf.at[1], load_sem.at[4]),
         pltpu.make_async_copy(v_in, ybuf.at[2], load_sem.at[5]),
+        pltpu.make_async_copy(w_in, wbuf, load_sem.at[6]),
     ]
 
     def zx(row, col):
@@ -128,25 +137,28 @@
     def xz(col, row):
         return row * nx + col
 
-    def p_slot(owner, which):
-        return pfull.at[:, pl.ds(pl.multiple_of(owner * block + which * half, half), half), :]
-
-    def mate_copy(owner, which):
+    def p_slot(j, owner, which):
+        return pfull.at[j, pl.ds(pl.multiple_of(owner * block + which * half, half), half), :]
+
+    def mate_copy(j, owner, which):
         return pltpu.make_async_remote_copy(
-            src_ref=p_slot(owner, which),
-            dst_ref=p_slot(owner, which),
-            send_sem=d_send.at[owner],
-            recv_sem=d_recv.at[owner],
+            src_ref=p_slot(j, owner, which),
+            dst_ref=p_slot(j, owner, which),
+            send_sem=d_send.at[j, owner],
+            recv_sem=d_recv.at[j, owner],
             device_id={"tp": mate},
             device_id_type=MESH,
         )
 
-    factors = Relay(
-        p_in.at[:, pl.ds(pl.multiple_of(core * half, half), half), :],
-        lambda owner: p_slot(owner, core),
-        p_send, p_recv, (z, nz), (x, nx), zx,
-        hook=lambda owner: mate_copy(owner, core).start(),
-    )
+    def factor_piece(j):
+        return Relay(
+            p_in.at[j, pl.ds(pl.multiple_of(core * half, half), half), :],
+            lambda owner: p_slot(j, owner, core),
+            p_send.at[j], p_recv.at[j], (z, nz), (x, nx), zx,
+            hook=lambda owner: mate_copy(j, owner, core).start(),
+        )
+
+    factors = [factor_piece(j) for j in range(3)]
 
     def w_piece(index, j, low, size, across):
         def slot(owner):
@@ -154,33 +166,38 @@
 
         first, second, dev = ((x, nx), (z, nz), xz) if across else ((z, nz), (x, nx), zx)
         return Relay(
-            w_in.at[j, pl.ds(low, size), :], slot, w_send.at[index], w_recv.at[index], first, second, dev
+            w16.at[j, pl.ds(low, size), :], slot, w_send.at[index], w_recv.at[index], first, second, dev
         )
 
     weights = [
-        w_piece(0, 0, 0, block, False),
-        w_piece(1, 1, 0, block, False),
-        w_piece(2, 2, 0, half, False),
-        w_piece(3, 2, half, half, True),
+        w_piece(2 * j + h, j, h * half, half, 2 * j + h == 5) for j in range(3) for h in range(2)
     ]
+    order = sorted(
+        (stage + PITCH * index, index) for index, piece in enumerate(weights) for stage in range(len(piece.steps))
+    )
+
+    def carry(count):
+        for _ in range(min(count, len(order))):
+            weights[order.pop(0)[1]].tick()
 
     def n_slot(owner):
         return nmfull.at[:, pl.ds(pl.multiple_of(owner * rr, rr), rr), :]
 
     momentum = Relay(n_slot(me), n_slot, n_send, n_recv, (z, nz), (x, nx), zx)
 
-    factors.tick()
     for load in loads:
         load.start()
-    factors.tick(2)
-    weights[0].tick()
-    factors.finish()
-    weights[0].tick()
-    weights[3].tick()
-    loads[0].wait()
-    for m in range(1, nfs):
-        owner = lax.rem(me + m, nfs)
-        mate_copy(owner, 1 - core).wait_recv()
+    pl.semaphore_wait(barrier, nfs + ntp - 2)
+    for piece in factors:
+        piece.tick()
+    loads[6].wait()
+    w16[...] = wbuf[...].astype(BF16)
+    for _ in range(nz - 2):
+        for piece in factors:
+            piece.tick()
+    factors[0].tick()
+    factors[1].tick()
+    carry(PACE[0])
 
     tokens = xbuf.shape[1]
     tile = min(256, tokens)
@@ -209,29 +226,34 @@
 
         sbuf[j] = sacc[...].astype(BF16)
 
+    def ready(j):
+        factors[j].finish()
+        for m in range(1, nfs):
+            mate_copy(j, lax.rem(me + m, nfs), 1 - core).wait_recv()
+
+    def scatter(j):
+        for m in range(1, nfs):
+            scatter_copy(j, m).start()
+
+    loads[0].wait()
     loads[1].wait()
     loads[2].wait()
+    ready(0)
     project(0, 0)
-    weights[0].tick()
-    weights[3].tick()
-    for m in range(1, nfs):
-        scatter_copy(0, m).start()
-    weights[1].tick()
+    scatter(0)
+    factors[2].tick()
+    carry(PACE[1])
     loads[3].wait()
+    ready(1)
     project(1, 0)
-    for m in range(1, nfs):
-        scatter_copy(1, m).start()
-    weights[0].tick()
-    weights[1].tick()
-    weights[3].tick()
+    scatter(1)
+    carry(PACE[2])
     loads[4].wait()
     loads[5].wait()
+    ready(2)
     project(2, 1)
-    for m in range(1, nfs):
-        scatter_copy(2, m).start()
-    weights[2].tick()
-    weights[1].tick()
-    weights[3].tick()
+    scatter(2)
+    carry(PACE[3])
 
     squares = jnp.zeros((), F32)
     for j in range(3):
@@ -259,6 +281,9 @@
     momentum.tick()
     for m in range(1, nfs):
         spread(tbuf, t_send, t_recv, "fs", nfs, m).start()
+    carry(PACE[4])
+    momentum.tick()
+    carry(PACE[5])
     momentum.tick()
     part = tbuf[0]
     for m in range(1, nfs):
@@ -267,37 +292,33 @@
     ubuf[0] = part
     for m in range(1, ntp):
         spread(ubuf, u_send, u_recv, "tp", ntp, m).start()
+    carry(PACE[6])
     momentum.tick()
-    weights[1].tick()
-    weights[2].tick()
-    momentum.tick()
-    weights[3].tick()
-    weights[2].tick()
+    carry(PACE[7])
     whole = part
     for m in range(1, ntp):
         spread(ubuf, u_send, u_recv, "tp", ntp, m).wait_recv()
         whole = whole + ubuf[m]
     total[...] = whole
-    weights[2].tick()
     momentum.finish()
-    for piece in weights:
-        piece.finish()
-
-    factors.drain()
+    carry(len(order))
+
+    for piece in factors:
+        piece.drain()
     momentum.drain()
     for piece in weights:
         piece.drain()
     for m in range(1, nfs):
         owner = lax.rem(me + m, nfs)
-        mate_copy(owner, core).wait_send()
         for j in range(3):
+            mate_copy(j, owner, core).wait_send()
             scatter_copy(j, m).wait_send()
         spread(tbuf, t_send, t_recv, "fs", nfs, m).wait_send()
     for m in range(1, ntp):
         spread(ubuf, u_send, u_recv, "tp", ntp, m).wait_send()
 
 
-def exchange(nfs, ntp, x, o, q, k, v, w16, p, m):
+def exchange(nfs, ntp, x, o, q, k, v, w, p, m):
     block, rank = p.shape[1], p.shape[2]
     rr, cols = m.shape[1], m.shape[2]
     tokens, model = x.shape
@@ -318,24 +339,26 @@
         scratch_shapes=[
             pltpu.VMEM((2, tokens, model), BF16),
             pltpu.VMEM((3, tokens, cols), BF16),
+            pltpu.VMEM(w.shape, F32),
+            pltpu.VMEM(w.shape, BF16),
             pltpu.VMEM((rank, cols), F32),
             pltpu.VMEM((3, rank, cols), BF16),
             pltpu.VMEM((nfs, 3, rr, cols), BF16),
             pltpu.VMEM((nfs, 8, 128), F32),
             pltpu.VMEM((ntp, 8, 128), F32),
-            dma((6,)),
-            dma((nfs, 4)), dma((nfs,)),
-            dma((nfs,)), dma((nfs,)),
-            dma((4, nfs, 4)), dma((4, nfs)),
+            dma((7,)),
+            dma((3, nfs, 4)), dma((3, nfs)),
+            dma((3, nfs)), dma((3, nfs)),
+            dma((6, nfs, 4)), dma((6, nfs)),
             dma((nfs, 4)), dma((nfs,)),
             dma((nfs, 3)), dma((nfs, 3)),
             dma((nfs,)), dma((nfs,)),
             dma((ntp,)), dma((ntp,)),
         ],
-        compiler_params=pltpu.CompilerParams(has_side_effects=True, vmem_limit_bytes=56 * 2**20),
+        compiler_params=pltpu.CompilerParams(collective_id=0, has_side_effects=True, vmem_limit_bytes=56 * 2**20),
         cost_estimate=pl.CostEstimate(flops=8 * 10**9, bytes_accessed=40 * 10**6, transcendentals=0),
         name="exchange",
-    )(x, o, q, k, v, w16, p, m)
+    )(x, o, q, k, v, w, p, m)
 
 
 def update_kernel(nfs, entries, w_ref, p_ref, n_ref, t_ref, master_ref, m_ref, nw_ref, copies_ref, steps_ref, mo_ref):
@@ -385,7 +408,7 @@
     nfs, ntp = mesh.shape["fs"], mesh.shape["tp"]
 
     def on_device(x, o, q, k, v, master, p, m):
-        wfull, pfull, nmfull, new_m, total = exchange(nfs, ntp, x, o, q, k, v, master.astype(BF16), p, m)
+        wfull, pfull, nmfull, new_m, total = exchange(nfs, ntp, x, o, q, k, v, master, p, m)
         return update(nfs, ntp, wfull, pfull, nmfull, total, master, new_m)
 
     in_specs = (

time: 144 us -> 128 us (0.89)
  Pallas kernels: 141 us -> 127 us
  other arithmetic: 2.39 us -> 0 us
    pallas_call x1, Pallas kernels: 127 us -> 114 us  [exchange(): pl.pallas_call(functools.partial(exchange_kernel, nfs, ntp), out_shape=(j...]
    convert_element_type x1 -> x0, other arithmetic: 2.39 us -> none  [on_device(): master.astype(BF16)]
where the time goes in v2:
time: 128 us
  Pallas kernels  127 us (99%)
    pallas_call x1, Pallas kernels, exchange(): pl.pallas_call(functools.partial(exchange_kernel, nfs, ntp), out_shape=(j...  114 us
    pallas_call x1, Pallas kernels, update(): pl.pallas_call(functools.partial(update_kernel, nfs, entries), grid=(nfs,...  13.5 us

profile of v2, /device:TPU:0, one launch (start us, length us, event | category | flops | bytes accessed | tf_op | source)
XLA Modules:
  0.0 127.7 jit_solution(5004240495978019238)
XLA Ops:
  0.6 113.5 %exchange.1 = (bf16[3,2048,512]{2,1,0:T(8,128)(2,1)}, bf16[3,2048,256]{2,1,0:T(8,128)(2,1)}, bf16[3,256,512]{2,1,0:T(8,128)(2,1)}, f32[3,32,512]{2,1,0:T(8,128)}, f32[8,128]{1,0:T(8,128)}) custom-call(bf16[2048,2048]{1,0:T(8,128)(2,1)} %x_in.1, bf16[2048,2048]{1,0:T(8,128)(2,1)} %o_in.1, bf16[2048,512]{1,0:T(8,128)(2,1)} %q_in.1, bf16[2048,512]{1,0:T(8,128)(2,1)} %k_in.1, ...), custom_call_target="tpu_custom_call" | custom-call | flops 8000000000 | bytes 40000000 | tf_op jit(solution)/shard_map/exchange/pallas_call | solution.py:328
  114.2 13.5 %update.1 = (f32[3,256,512]{2,1,0:T(8,128)}, bf16[3,2048,512]{2,1,0:T(8,128)(2,1)}, f32[3,256,512]{2,1,0:T(8,128)}, f32[3,32,512]{2,1,0:T(8,128)}) custom-call(bf16[3,2048,512]{2,1,0:T(8,128)(2,1)} %get-tuple-element.9.w_ref, bf16[3,2048,256]{2,1,0:T(8,128)(2,1)} %get-tuple-element.10.p_ref, bf16[3,256,512]{2,1,0:T(8,128)(2,1)} %get-tuple-element.11.n_ref, ...), custom_call_target="tpu_custom_call" | custom-call | flops 2000000000 | bytes 20000000 | tf_op jit(solution)/shard_map/update/pallas_call | solution.py:390
